TPU v7x, 32 devices: a whole 2x2x4 slice. The times are simulated.
32 devices in a mesh: dp: 4 (over y, x), kv: 4 (over z), tp: 2 (over core).
Axes of the slice: x: 2, y: 2, z: 4, core: 2. Of those that a mesh axis runs over, the one named last changes fastest.
Arguments:
- tokens: bfloat16 [128, 2048], P('dp', ('kv', 'tp')), may hold values from -60 to 60
- first_norm_gain: float32 [2048], replicated, may hold values from 0.1 to 1.9
- first_gate_weight: bfloat16 [2048, 5632], P(None, ('kv', 'tp')), may hold values from -0.125 to 0.125
- first_up_weight: bfloat16 [2048, 5632], P(None, ('kv', 'tp')), may hold values from -0.125 to 0.125
- first_down_weight: bfloat16 [5632, 2048], P(('kv', 'tp')), may hold values from -0.109375 to 0.109375
- mixer_norm_gain: float32 [2048], replicated, may hold values from 0.1 to 1.9
- query_weight: bfloat16 [2048, 1024], P('kv', 'tp'), may hold values from -0.125 to 0.125
- key_weight: bfloat16 [2048, 1024], P('kv', 'tp'), may hold values from -0.125 to 0.125
- value_weight: bfloat16 [2048, 1024], P('kv', 'tp'), may hold values from -0.125 to 0.125
- output_gate_weight: bfloat16 [2048, 1024], P('kv', 'tp'), may hold values from -0.125 to 0.125
- strength_weight: bfloat16 [2048, 8], replicated, may hold values from -0.125 to 0.125
- decay_weight: bfloat16 [2048, 8], replicated, may hold values from -0.125 to 0.125
- head_decay_log: float32 [8], replicated, may hold values from 0 to 2.77
- decay_input_bias: float32 [8], replicated, may hold values from -4 to 0
- decay_extra_log: float32 [128, 8], P(('dp', 'kv'), 'tp'), may hold values from -0.7 to 0
- head_norm_gain: float32 [128], replicated, may hold values from 0.1 to 1.9
- state: float32 [128, 8, 128, 128], P(('dp', 'kv'), 'tp'), may hold values from -0.6 to 0.6
- mixer_output_weight: bfloat16 [1024, 2048], P('tp', 'kv'), may hold values from -0.1875 to 0.1875
- second_norm_gain: float32 [2048], replicated, may hold values from 0.1 to 1.9
- second_gate_weight: bfloat16 [2048, 5632], P(None, ('kv', 'tp')), may hold values from -0.125 to 0.125
- second_up_weight: bfloat16 [2048, 5632], P(None, ('kv', 'tp')), may hold values from -0.125 to 0.125
- second_down_weight: bfloat16 [5632, 2048], P(('kv', 'tp')), may hold values from -0.109375 to 0.109375
Outputs:
- layer_out: bfloat16 [128, 2048], P('dp', ('kv', 'tp'))
- new_state: float32 [128, 8, 128, 128], P(('dp', 'kv'), 'tp')
All inputs are finite; a program needn't handle non-finite values.
Results may differ from a plain program's by a relative error of at most 0.014.
Values may be sent and summed in bfloat16 or wider, within the bound.
A program may use at most 64 MiB of HBM per device.

v0:
```python
import jax
import jax.numpy as jnp
from jax import lax
from jax.sharding import PartitionSpec as P

EPS = 1e-06


def row_scale(values):
    return lax.rsqrt(jnp.mean(values * values, axis=-1, keepdims=True) + EPS)


def unit_rows(values):
    return values * lax.rsqrt(jnp.sum(values * values, axis=-1, keepdims=True) + EPS)


def block_terms(row_data, gain_vec, w_gate, w_up, w_down):
    rows32 = row_data.astype(jnp.float32)
    normed = (rows32 * row_scale(rows32) * gain_vec).astype(jnp.bfloat16)
    gate_pre = jnp.dot(normed, w_gate, preferred_element_type=jnp.float32)
    upward = jnp.dot(normed, w_up, preferred_element_type=jnp.float32)
    hidden = (jax.nn.silu(gate_pre) * upward).astype(jnp.bfloat16)
    return jnp.dot(hidden, w_down, preferred_element_type=jnp.float32)


def delta_step(
    query_vec, key_vec, value_vec, gate_vals, beta_gate, head_decay_rate, state, head_norm_gain
):
    recalled = jnp.einsum("shd,shde->she", key_vec, state, precision=lax.Precision.HIGHEST)
    correction = beta_gate[..., None] * (value_vec - head_decay_rate[..., None] * recalled)
    new_state = (
        head_decay_rate[..., None, None] * state + key_vec[..., :, None] * correction[..., None, :]
    )
    read_out = jnp.einsum("shd,shde->she", query_vec, new_state, precision=lax.Precision.HIGHEST)
    normed = read_out * row_scale(read_out) * head_norm_gain
    return (normed * jax.nn.silu(gate_vals), new_state)


def shards(
    tokens,
    first_norm_gain,
    first_gate_weight,
    first_up_weight,
    first_down_weight,
    mixer_norm_gain,
    query_weight,
    key_weight,
    value_weight,
    output_gate_weight,
    strength_weight,
    decay_weight,
    head_decay_log,
    decay_input_bias,
    decay_extra_log,
    head_norm_gain,
    state,
    mixer_output_weight,
    second_norm_gain,
    second_gate_weight,
    second_up_weight,
    second_down_weight,
):
    batch_rows, columns = tokens.shape
    kv_index = lax.axis_index("kv")
    tp_index = lax.axis_index("tp")
    own_block = kv_index * lax.axis_size("tp") + tp_index
    seq_dev, heads_dev, head_size = (state.shape[0], state.shape[1], state.shape[2])
    kv_width = query_weight.shape[0]
    head_cols = heads_dev * head_size
    model_width = mixer_norm_gain.shape[0]
    rows_all = lax.all_gather(tokens, ("kv", "tp"), axis=1, tiled=True)
    ffn_terms = block_terms(
        rows_all, first_norm_gain, first_gate_weight, first_up_weight, first_down_weight
    )
    share_sum = lax.psum_scatter(
        ffn_terms.astype(jnp.bfloat16), ("kv", "tp"), scatter_dimension=1, tiled=True
    ).astype(jnp.float32)
    first_rows = (tokens.astype(jnp.float32) + 0.5 * share_sum).astype(jnp.bfloat16)
    first32 = first_rows.astype(jnp.float32)
    kv_block = lax.all_gather(first_rows, "tp", axis=1, tiled=True)
    own_gain = lax.dynamic_slice_in_dim(mixer_norm_gain, own_block * columns, columns)
    own_scaled = (first32 * own_gain).astype(jnp.bfloat16)
    beta_rows = lax.dynamic_slice_in_dim(strength_weight, own_block * columns, columns, 0)
    decay_rows = lax.dynamic_slice_in_dim(decay_weight, own_block * columns, columns, 0)
    squares, beta_pre, decay_logits = lax.psum(
        (
            jnp.sum(first32 * first32, axis=1),
            jnp.dot(own_scaled, beta_rows, preferred_element_type=jnp.float32),
            jnp.dot(own_scaled, decay_rows, preferred_element_type=jnp.float32),
        ),
        ("kv", "tp"),
    )
    row_factor = lax.rsqrt(squares / model_width + EPS)
    block_gain = lax.dynamic_slice_in_dim(mixer_norm_gain, kv_index * kv_width, kv_width)
    block_scaled = (kv_block.astype(jnp.float32) * block_gain).astype(jnp.bfloat16)
    projected = lax.psum_scatter(
        jnp.concatenate(
            [
                jnp.dot(block_scaled, weight, preferred_element_type=jnp.float32)
                for weight in (query_weight, key_weight, value_weight, output_gate_weight)
            ],
            axis=1,
        ).astype(jnp.bfloat16),
        "kv",
        scatter_dimension=0,
        tiled=True,
    ).astype(jnp.float32)
    own_rows = kv_index * seq_dev
    own_factor = lax.dynamic_slice_in_dim(row_factor, own_rows, seq_dev)[:, None]
    projected = projected * own_factor

    def split_heads(role_index):
        return projected[:, role_index * head_cols : (role_index + 1) * head_cols].reshape(
            seq_dev, heads_dev, head_size
        )

    query_vec = unit_rows(jax.nn.silu(split_heads(0))) * head_size ** (-0.5)
    key_vec = unit_rows(jax.nn.silu(split_heads(1)))
    value_vec = jax.nn.silu(split_heads(2))
    gate_vals = split_heads(3)
    head_start = tp_index * heads_dev

    def local_gate_values(values):
        own_seqs = lax.dynamic_slice_in_dim(values, own_rows, seq_dev, 0)
        return lax.dynamic_slice_in_dim(own_seqs, head_start, heads_dev, 1) * own_factor

    beta_gate = jax.nn.sigmoid(local_gate_values(beta_pre))
    decay_log_term = lax.dynamic_slice_in_dim(head_decay_log, head_start, heads_dev)
    decay_offset_term = lax.dynamic_slice_in_dim(decay_input_bias, head_start, heads_dev)
    head_decay_rate = jnp.exp(
        decay_extra_log
        - jnp.exp(decay_log_term)
        * jax.nn.softplus(local_gate_values(decay_logits) + decay_offset_term)
    )
    heads_f32, new_state = delta_step(
        query_vec, key_vec, value_vec, gate_vals, beta_gate, head_decay_rate, state, head_norm_gain
    )
    heads_out = heads_f32.reshape(seq_dev, head_cols).astype(jnp.bfloat16)
    mixer_terms = jnp.dot(
        lax.all_gather(heads_out, "kv", axis=0, tiled=True),
        mixer_output_weight,
        preferred_element_type=jnp.float32,
    )
    mixer_sum = lax.psum_scatter(
        mixer_terms.astype(jnp.bfloat16), "tp", scatter_dimension=1, tiled=True
    ).astype(jnp.float32)
    second_rows = (first32 + mixer_sum).astype(jnp.bfloat16)
    rows_last = lax.all_gather(second_rows, ("kv", "tp"), axis=1, tiled=True)
    last_terms = block_terms(
        rows_last, second_norm_gain, second_gate_weight, second_up_weight, second_down_weight
    )
    last_sum = lax.psum_scatter(
        last_terms.astype(jnp.bfloat16), ("kv", "tp"), scatter_dimension=1, tiled=True
    ).astype(jnp.float32)
    layer_out = (second_rows.astype(jnp.float32) + 0.5 * last_sum).astype(jnp.bfloat16)
    return (layer_out, new_state)


def solution(mesh):
    placed = (
        P("dp", ("kv", "tp")),
        P(),
        P(None, ("kv", "tp")),
        P(None, ("kv", "tp")),
        P(("kv", "tp"), None),
        P(),
        P("kv", "tp"),
        P("kv", "tp"),
        P("kv", "tp"),
        P("kv", "tp"),
        P(),
        P(),
        P(),
        P(),
        P(("dp", "kv"), "tp"),
        P(),
        P(("dp", "kv"), "tp", None, None),
        P("tp", "kv"),
        P(),
        P(None, ("kv", "tp")),
        P(None, ("kv", "tp")),
        P(("kv", "tp"), None),
    )
    return jax.shard_map(
        shards,
        mesh=mesh,
        in_specs=placed,
        out_specs=(P("dp", ("kv", "tp")), P(("dp", "kv"), "tp", None, None)),
        check_vma=False,
    )
```

profile of v0, /device:TPU:0, one launch (start us, length us, event | category | flops | bytes accessed | tf_op | source)
XLA Modules:
  0.0 181.2 jit_solution(4792796293112144642)
XLA Ops:
  7.2 16.1 %all_gather.12 = bf16[32,2048]{1,0:T(8,128)(2,1)S(1)} all-gather(bf16[32,256]{1,0:T(8,128)(2,1)} %param.22), channel_id=1, replica_groups=mesh['dp'=4,'kv'=4,'tp'=2] {'kv','tp'}, dimensions={1}, use_global_device_ids=true | all-gather | bytes 147456 | tf_op jit(solution)/shard_map/all_gather | solution.py:71
  23.3 0.1 fusion.2
  23.5 0.5 copy-done.8
  24.0 3.4 %fusion.26 = f32[32,704]{1,0:T(8,128)} fusion(bf16[2048,704]{0,1:T(8,128)(2,1)} %param.24, bf16[32,2048]{1,0:T(8,128)(2,1)S(1)} %all_gather.12, f32[2048]{0:T(1024)} %param.23, f32[32]{0:T(128)S(1)} %add_rsqrt_fusion.5), kind=kOutput, calls=%fused_computation.41 | convolution fusion | flops 92536832 | bytes 3113088 | tf_op jit(solution)/shard_map/dot_general | solution.py:20
  27.4 4.3 %convolution_convert_fusion.1 = bf16[32,2048]{1,0:T(8,128)(2,1)} fusion(bf16[704,2048]{1,0:T(8,128)(2,1)S(1)} %copy-done, bf16[2048,704]{0,1:T(8,128)(2,1)} %param.25, f32[32,704]{1,0:T(8,128)} %fusion.26, bf16[32,2048]{1,0:T(8,128)(2,1)S(1)} %all_gather.12, f32[2048]{0:T(1024)} %param.23, f32[32]{0:T(128)} %copy-done.8), kind=kOutput, calls=%fused_computation.1 | convolution fusion | flops 185012224 | bytes 6127744 | tf_op jit(solution)/shard_map/dot_general | solution.py:23
  31.7 0.0 reduce-scatter.7.cloned.1.call-start
  31.8 0.7 dynamic_slice.35
  32.5 0.8 dynamic_slice.32
  33.3 0.8 dynamic_slice.29
  34.0 0.7 dynamic-slice_exponential_fusion
  34.8 28.7 %reduce-scatter.5.cloned.1.call-done = bf16[32,256]{1,0:T(8,128)(2,1)} async-done(((bf16[32,2048]{1,0:T(8,128)(2,1)}), bf16[32,256]{1,0:T(8,128)(2,1)}) %reduce-scatter.5.cloned.1.call-update) | async-done | bytes 16400 | tf_op jit(solution)/shard_map/reduce_scatter | solution.py:75
  63.5 0.8 fusion.28
  64.3 1.8 %all_gather.13 = bf16[32,512]{1,0:T(8,128)(2,1)S(1)} all-gather(bf16[32,256]{1,0:T(8,128)(2,1)S(1)} %get-tuple-element.8), channel_id=1, replica_groups=mesh['dp'=4,'kv'=4,'tp'=2] {'tp'}, dimensions={1}, use_global_device_ids=true | all-gather | bytes 49152 | tf_op jit(solution)/shard_map/all_gather | solution.py:80
  66.2 0.8 fusion.43
  67.0 0.8 fusion.41
  67.8 0.2 convolution_convert_fusion.5
  68.0 1.2 convolution_convert_fusion.4
  69.2 1.2 convolution_convert_fusion.3
  70.5 1.3 convolution_convert_fusion.6
  71.7 0.7 pad_maximum_fusion
  72.4 0.0 reduce-scatter.9.cloned.1.call-start
  72.5 14.4 %all-reduce = (f32[32]{0:T(128)S(1)}, f32[32,8]{0,1:T(8,128)S(1)}, f32[32,8]{0,1:T(8,128)S(1)}) all-reduce(f32[32]{0:T(128)S(1)} %get-tuple-element.7, f32[32,8]{0,1:T(8,128)S(1)} %fusion.43, f32[32,8]{0,1:T(8,128)S(1)} %fusion.41), channel_id=1, replica_groups=mesh['dp'=4,'kv'=4,'tp'=2] {'kv','tp'}, use_global_device_ids=true, to_apply=%region_4.5 | all-reduce | flops 544 | bytes 4352 | tf_op jit(solution)/shard_map/psum | solution.py:85
  86.8 0.1 dynamic_slice.30
  86.9 0.1 add_divide_fusion
  87.0 0.1 copy.24
  87.1 3.0 %reduce-scatter.7.cloned.1.call-done = bf16[8,2048]{1,0:T(8,128)(2,1)} async-done(((bf16[32,2048]{1,0:T(8,128)(2,1)}), bf16[8,2048]{1,0:T(8,128)(2,1)}) %reduce-scatter.7.cloned.1.call-update) | async-done | bytes 32784 | tf_op jit(solution)/shard_map/reduce_scatter | solution.py:96
  90.1 1.0 convert_multiply_fusion.4
  91.1 0.1 multiply_reduce_fusion.1
  91.2 0.1 fusion.69
  91.3 0.1 broadcast_multiply_fusion
  91.4 3.4 %fusion.39 = f32[8,4,1,128]{3,2,1,0:T(1,128)S(1)} fusion(f32[8,4,128,128]{3,2,1,0:T(8,128)} %param.38, f32[8,4,128,1]{2,0,1,3:T(8,128)S(1)} %fusion.69), kind=kOutput, calls=%fused_computation.62 | convolution fusion | flops 6291456 | bytes 2129920 | tf_op jit(solution)/shard_map/shd,shde->she/dot_general | solution.py:29
  94.8 0.1 multiply_bitcast_fusion
  94.9 0.8 multiply_add_fusion
  95.7 1.3 copy-done.2
  97.0 1.9 %fusion.37 = f32[8,4,1,128]{3,2,1,0:T(1,128)S(1)} fusion(f32[8,4,128,128]{3,2,1,0:T(8,128)S(1)} %multiply_add_fusion, f32[8,4,128,1]{2,0,1,3:T(8,128)S(1)} %get-tuple-element.9), kind=kOutput, calls=%fused_computation.60 | convolution fusion | flops 6291456 | bytes 2129920 | tf_op jit(solution)/shard_map/shd,shde->she/dot_general | solution.py:34
  98.9 0.1 fusion.31
  99.0 0.1 fusion.45
  99.1 13.1 %all_gather.14 = bf16[32,512]{1,0:T(8,128)(2,1)S(1)} all-gather(bf16[8,512]{1,0:T(8,128)(2,1)S(1)} %fusion.45), channel_id=1, replica_groups=mesh['dp'=4,'kv'=4,'tp'=2] {'kv'}, dimensions={0}, use_global_device_ids=true | all-gather | bytes 40960 | tf_op jit(solution)/shard_map/all_gather | solution.py:140
  112.2 0.8 convolution_convert_fusion.2
  113.0 0.0 reduce-scatter.11.cloned.1.call-start
  113.1 5.8 %reduce-scatter.9.cloned.1.call-done = bf16[32,256]{1,0:T(8,128)(2,1)} async-done(((bf16[32,512]{1,0:T(8,128)(2,1)}), bf16[32,256]{1,0:T(8,128)(2,1)}) %reduce-scatter.9.cloned.1.call-update) | async-done | bytes 16400 | tf_op jit(solution)/shard_map/reduce_scatter | solution.py:144
  118.8 0.7 fusion.30
  119.6 14.3 %all_gather.15 = bf16[32,2048]{1,0:T(8,128)(2,1)S(1)} all-gather(bf16[32,256]{1,0:T(8,128)(2,1)S(1)} %fusion.30), channel_id=1, replica_groups=mesh['dp'=4,'kv'=4,'tp'=2] {'kv','tp'}, dimensions={1}, use_global_device_ids=true | all-gather | bytes 147456 | tf_op jit(solution)/shard_map/all_gather | solution.py:148
  133.8 0.1 fusion.5
  134.0 2.7 %fusion.22 = f32[32,704]{1,0:T(8,128)S(1)} fusion(bf16[2048,704]{0,1:T(8,128)(2,1)} %param.41, bf16[32,2048]{1,0:T(8,128)(2,1)S(1)} %all_gather.15, f32[2048]{0:T(1024)S(1)} %copy-done.6, f32[32]{0:T(128)S(1)} %add_rsqrt_fusion.3), kind=kOutput, calls=%fused_computation.40 | convolution fusion | flops 92536832 | bytes 3113088 | tf_op jit(solution)/shard_map/dot_general | solution.py:20
  136.7 5.1 %convolution_convert_fusion = bf16[32,2048]{1,0:T(8,128)(2,1)} fusion(bf16[704,2048]{1,0:T(8,128)(2,1)} %param.43, bf16[2048,704]{0,1:T(8,128)(2,1)} %param.42, f32[32,704]{1,0:T(8,128)S(1)} %fusion.22, bf16[32,2048]{1,0:T(8,128)(2,1)S(1)} %all_gather.15, f32[2048]{0:T(1024)S(1)} %copy-done.6, f32[32]{0:T(128)S(1)} %add_rsqrt_fusion.3), kind=kOutput, calls=%fused_computation | convolution fusion | flops 185012224 | bytes 6127744 | tf_op jit(solution)/shard_map/dot_general | solution.py:23
  141.9 31.5 %reduce-scatter.11.cloned.1.call-done = bf16[32,256]{1,0:T(8,128)(2,1)} async-done(((bf16[32,2048]{1,0:T(8,128)(2,1)}), bf16[32,256]{1,0:T(8,128)(2,1)}) %reduce-scatter.11.cloned.1.call-update) | async-done | bytes 16400 | tf_op jit(solution)/shard_map/reduce_scatter | solution.py:152
  173.4 1.3 add_convert_fusion
  (30 shorter events, 0.2 us)
Async XLA Ops:
  7.2 20.2 %copy-start = (bf16[704,2048]{1,0:T(8,128)(2,1)S(1)}, bf16[704,2048]{1,0:T(8,128)(2,1)}, u32[]{:S(2)}) copy-start(bf16[704,2048]{1,0:T(8,128)(2,1)} %param.26) | copy-start | bytes 8650756
  7.2 56.3 %reduce-scatter.5.cloned.1.call-start = ((), (), s32[]{:S(2)}) async-start(), calls=%async_computation.4 | async-start | bytes 147456 | tf_op jit(solution)/shard_map/reduce_scatter | solution.py:75
  23.5 0.5 copy-start.8
  27.4 36.2 %copy-start.5 = (bf16[32,256]{1,0:T(8,128)(2,1)S(1)}, bf16[32,256]{1,0:T(8,128)(2,1)}, u32[]{:S(2)}) copy-start(bf16[32,256]{1,0:T(8,128)(2,1)} %param.22) | copy-start | bytes 49156
  27.4 40.4 %copy-start.3 = (bf16[512,512]{1,0:T(8,128)(2,1)S(1)}, bf16[512,512]{1,0:T(8,128)(2,1)}, u32[]{:S(2)}) copy-start(bf16[512,512]{1,0:T(8,128)(2,1)} %param.29) | copy-start | bytes 1572868
  31.7 55.2 %copy-start.7 = (f32[8,4]{0,1:T(4,128)S(1)}, f32[8,4]{0,1:T(4,128)}, u32[]{:S(2)}) copy-start(f32[8,4]{0,1:T(4,128)} %param.36) | copy-start | bytes 388
  31.7 58.4 %reduce-scatter.7.cloned.1.call-start = ((), (), s32[]{:S(2)}) async-start(), calls=%async_computation.5 | async-start | bytes 163840 | tf_op jit(solution)/shard_map/reduce_scatter | solution.py:96
  72.4 46.4 %reduce-scatter.9.cloned.1.call-start = ((), (), s32[]{:S(2)}) async-start(), calls=%async_computation.6 | async-start | bytes 49152 | tf_op jit(solution)/shard_map/reduce_scatter | solution.py:144
  90.1 4.8 %copy-start.1 = (f32[8,4,128,128]{3,2,1,0:T(8,128)S(1)}, f32[8,4,128,128]{3,2,1,0:T(8,128)}, u32[]{:S(2)}) copy-start(f32[8,4,128,128]{3,2,1,0:T(8,128)} %param.38) | copy-start | bytes 6291460
  94.9 4.1 %copy-start.9 = (f32[128]{0:T(128)S(1)}, f32[128]{0:T(128)}, u32[]{:S(2)}) copy-start(f32[128]{0:T(128)} %param.37) | copy-start | bytes 1540
  94.9 17.3 %copy-start.4 = (bf16[512,512]{1,0:T(8,128)(2,1)S(1)}, bf16[512,512]{1,0:T(8,128)(2,1)}, u32[]{:S(2)}) copy-start(bf16[512,512]{1,0:T(8,128)(2,1)} %param.39) | copy-start | bytes 1572868
  94.9 39.1 %copy-start.6 = (f32[2048]{0:T(1024)S(1)}, f32[2048]{0:T(1024)}, u32[]{:S(2)}) copy-start(f32[2048]{0:T(1024)} %param.40) | copy-start | bytes 24580
  95.7 1.3 copy-start.2
  113.0 60.3 %reduce-scatter.11.cloned.1.call-start = ((), (), s32[]{:S(2)}) async-start(), calls=%async_computation.7 | async-start | bytes 147456 | tf_op jit(solution)/shard_map/reduce_scatter | solution.py:152
Sparse Core Ops, SparseCore 0:
  31.8 31.6 reduce-scatter.4
  72.5 17.5 reduce-scatter.6
  113.2 5.6 reduce-scatter.8
  142.0 31.3 reduce-scatter.10
where the time goes:
time: 182 us; the launch traced here: 181 us
  waiting for transfers between devices  69.1 us (38%)
  blocking collectives  59.7 us (33%)
  matrix products  27.2 us (15%)
  between operations  13.9 us (8%)
  other arithmetic  6.18 us (3%)
  local copies, waits for them, and re-layouts  5.02 us (3%)
    reduce_scatter x1, waiting for transfers between devices, shards(): lax.psum_scatter(last_terms.astype(jnp.bfloat16), ('kv', 'tp'), scatter_d...  31.5 us
    reduce_scatter x1, waiting for transfers between devices, shards(): lax.psum_scatter(ffn_terms.astype(jnp.bfloat16), ('kv', 'tp'), scatter_di...  28.7 us
    all_gather x1, blocking collectives, shards(): rows_all = lax.all_gather(tokens, ('kv', 'tp'), axis=1, tiled=True)  16.1 us
    psum x1, blocking collectives, shards(): lax.psum((jnp.sum(first32 * first32, axis=1), jnp.dot(own_scaled, beta_ro...  14.4 us
    all_gather x1, blocking collectives, shards(): rows_last = lax.all_gather(second_rows, ('kv', 'tp'), axis=1, tiled=True)  14.3 us
    all_gather x1, blocking collectives, shards(): lax.all_gather(heads_out, 'kv', axis=0, tiled=True)  13.1 us
    dot_general x2, matrix products, block_terms(): return jnp.dot(hidden, w_down, preferred_element_type=jnp.float32)  9.45 us
    dot_general x2, matrix products, block_terms(): gate_pre = jnp.dot(normed, w_gate, preferred_element_type=jnp.float32)  6.1 us
  transfers between devices with their start and end apart: 4, of which 4 were waited for; matrix products, arithmetic and copies ran while one was open for 2% of the time, Pallas kernels for 0%

commit v1 on v0

--- a/solution.py
+++ b/solution.py
@@ -83,12 +83,15 @@
     beta_rows = lax.dynamic_slice_in_dim(strength_weight, own_block * columns, columns, 0)
     decay_rows = lax.dynamic_slice_in_dim(decay_weight, own_block * columns, columns, 0)
     squares, beta_pre, decay_logits = lax.psum(
-        (
-            jnp.sum(first32 * first32, axis=1),
-            jnp.dot(own_scaled, beta_rows, preferred_element_type=jnp.float32),
-            jnp.dot(own_scaled, decay_rows, preferred_element_type=jnp.float32),
+        lax.psum(
+            (
+                jnp.sum(first32 * first32, axis=1),
+                jnp.dot(own_scaled, beta_rows, preferred_element_type=jnp.float32),
+                jnp.dot(own_scaled, decay_rows, preferred_element_type=jnp.float32),
+            ),
+            "tp",
         ),
-        ("kv", "tp"),
+        "kv",
     )
     row_factor = lax.rsqrt(squares / model_width + EPS)
     block_gain = lax.dynamic_slice_in_dim(mixer_norm_gain, kv_index * kv_width, kv_width)

time: 182 us -> 182 us (level)
  waiting for transfers between devices: 69.1 us -> 72.2 us
  blocking collectives: 59.7 us -> 56.7 us
    psum x1, blocking collectives: 14.4 us -> 2.52 us  [shards(): lax.psum((jnp.sum(first32 * first32, axis=1), jnp.dot(own_scaled, beta_ro...]
    psum x0 -> x1, blocking collectives: none -> 8.94 us  [shards(): lax.psum(lax.psum((jnp.sum(first32 * first32, axis=1), jnp.dot(own_scaled...]
    reduce_scatter x1, waiting for transfers between devices: 3 us -> 6.02 us  [shards(): lax.psum_scatter(jnp.concatenate([jnp.dot(block_scaled, weight, preferred...]
where the time goes in v1:
time: 182 us; the launch traced here: 181 us
  waiting for transfers between devices  72.2 us (40%)
  blocking collectives  56.7 us (31%)
  matrix products  27.2 us (15%)
  between operations  13.9 us (8%)
  other arithmetic  6.18 us (3%)
  local copies, waits for them, and re-layouts  5.02 us (3%)
    reduce_scatter x1, waiting for transfers between devices, shards(): lax.psum_scatter(last_terms.astype(jnp.bfloat16), ('kv', 'tp'), scatter_d...  31.6 us
    reduce_scatter x1, waiting for transfers between devices, shards(): lax.psum_scatter(ffn_terms.astype(jnp.bfloat16), ('kv', 'tp'), scatter_di...  28.7 us
    all_gather x1, blocking collectives, shards(): rows_all = lax.all_gather(tokens, ('kv', 'tp'), axis=1, tiled=True)  16.1 us
    all_gather x1, blocking collectives, shards(): rows_last = lax.all_gather(second_rows, ('kv', 'tp'), axis=1, tiled=True)  14.2 us
    all_gather x1, blocking collectives, shards(): lax.all_gather(heads_out, 'kv', axis=0, tiled=True)  13.1 us
    dot_general x2, matrix products, block_terms(): return jnp.dot(hidden, w_down, preferred_element_type=jnp.float32)  9.45 us
    psum x1, blocking collectives, shards(): lax.psum(lax.psum((jnp.sum(first32 * first32, axis=1), jnp.dot(own_scaled...  8.94 us
    dot_general x2, matrix products, block_terms(): gate_pre = jnp.dot(normed, w_gate, preferred_element_type=jnp.float32)  6.11 us
  transfers between devices with their start and end apart: 4, of which 4 were waited for; matrix products, arithmetic and copies ran while one was open for 2% of the time, Pallas kernels for 0%

profile of v1, /device:TPU:0, one launch (start us, length us, event | category | flops | bytes accessed | tf_op | source)
XLA Modules:
  0.0 181.4 jit_solution(8419079967942011750)
XLA Ops:
  7.2 16.1 %all_gather.12 = bf16[32,2048]{1,0:T(8,128)(2,1)S(1)} all-gather(bf16[32,256]{1,0:T(8,128)(2,1)} %param.22), channel_id=1, replica_groups=mesh['dp'=4,'kv'=4,'tp'=2] {'kv','tp'}, dimensions={1}, use_global_device_ids=true | all-gather | bytes 147456 | tf_op jit(solution)/shard_map/all_gather | solution.py:71
  23.3 0.1 fusion.2
  23.5 0.5 copy-done.8
  24.0 3.4 %fusion.26 = f32[32,704]{1,0:T(8,128)} fusion(bf16[2048,704]{0,1:T(8,128)(2,1)} %param.24, bf16[32,2048]{1,0:T(8,128)(2,1)S(1)} %all_gather.12, f32[2048]{0:T(1024)} %param.23, f32[32]{0:T(128)S(1)} %add_rsqrt_fusion.5), kind=kOutput, calls=%fused_computation.41 | convolution fusion | flops 92536832 | bytes 3113088 | tf_op jit(solution)/shard_map/dot_general | solution.py:20
  27.4 4.3 %convolution_convert_fusion.1 = bf16[32,2048]{1,0:T(8,128)(2,1)} fusion(bf16[704,2048]{1,0:T(8,128)(2,1)S(1)} %copy-done, bf16[2048,704]{0,1:T(8,128)(2,1)} %param.25, f32[32,704]{1,0:T(8,128)} %fusion.26, bf16[32,2048]{1,0:T(8,128)(2,1)S(1)} %all_gather.12, f32[2048]{0:T(1024)} %param.23, f32[32]{0:T(128)} %copy-done.8), kind=kOutput, calls=%fused_computation.1 | convolution fusion | flops 185012224 | bytes 6127744 | tf_op jit(solution)/shard_map/dot_general | solution.py:23
  31.7 0.0 reduce-scatter.7.cloned.1.call-start
  31.8 0.7 dynamic_slice.35
  32.5 0.8 dynamic_slice.32
  33.3 0.8 dynamic_slice.29
  34.0 0.7 dynamic-slice_exponential_fusion
  34.8 28.7 %reduce-scatter.5.cloned.1.call-done = bf16[32,256]{1,0:T(8,128)(2,1)} async-done(((bf16[32,2048]{1,0:T(8,128)(2,1)}), bf16[32,256]{1,0:T(8,128)(2,1)}) %reduce-scatter.5.cloned.1.call-update) | async-done | bytes 16400 | tf_op jit(solution)/shard_map/reduce_scatter | solution.py:75
  63.5 0.8 fusion.28
  64.3 1.8 %all_gather.13 = bf16[32,512]{1,0:T(8,128)(2,1)S(1)} all-gather(bf16[32,256]{1,0:T(8,128)(2,1)S(1)} %get-tuple-element.11), channel_id=1, replica_groups=mesh['dp'=4,'kv'=4,'tp'=2] {'tp'}, dimensions={1}, use_global_device_ids=true | all-gather | bytes 49152 | tf_op jit(solution)/shard_map/all_gather | solution.py:80
  66.2 0.8 fusion.43
  67.0 0.8 fusion.41
  67.8 0.2 convolution_convert_fusion.5
  68.0 1.2 convolution_convert_fusion.4
  69.2 1.2 convolution_convert_fusion.3
  70.5 1.3 convolution_convert_fusion.6
  71.7 0.7 pad_maximum_fusion
  72.4 0.0 reduce-scatter.9.cloned.1.call-start
  72.5 2.5 %all-reduce.1 = (f32[32]{0:T(128)S(1)}, f32[32,8]{0,1:T(8,128)S(1)}, f32[32,8]{0,1:T(8,128)S(1)}) all-reduce(f32[32]{0:T(128)S(1)} %get-tuple-element.10, f32[32,8]{0,1:T(8,128)S(1)} %fusion.43, f32[32,8]{0,1:T(8,128)S(1)} %fusion.41), channel_id=1, replica_groups=mesh['dp'=4,'kv'=4,'tp'=2] {'tp'}, use_global_device_ids=true, to_apply=%region_4.5 | all-reduce | flops 544 | bytes 4352 | tf_op jit(solution)/shard_map/psum | solution.py:86
  75.0 8.9 %all-reduce = (f32[32]{0:T(128)S(1)}, f32[32,8]{0,1:T(8,128)S(1)}, f32[32,8]{0,1:T(8,128)S(1)}) all-reduce(f32[32]{0:T(128)S(1)} %get-tuple-element.7, f32[32,8]{0,1:T(8,128)S(1)} %get-tuple-element.8, f32[32,8]{0,1:T(8,128)S(1)} %get-tuple-element.9), channel_id=1, replica_groups=mesh['dp'=4,'kv'=4,'tp'=2] {'kv'}, use_global_device_ids=true, to_apply=%region_5.6 | all-reduce | flops 544 | bytes 4352 | tf_op jit(solution)/shard_map/psum | solution.py:85
  83.9 0.1 dynamic_slice.30
  84.0 0.1 add_divide_fusion
  84.1 0.1 copy.24
  84.2 6.0 %reduce-scatter.7.cloned.1.call-done = bf16[8,2048]{1,0:T(8,128)(2,1)} async-done(((bf16[32,2048]{1,0:T(8,128)(2,1)}), bf16[8,2048]{1,0:T(8,128)(2,1)}) %reduce-scatter.7.cloned.1.call-update) | async-done | bytes 32784 | tf_op jit(solution)/shard_map/reduce_scatter | solution.py:99
  90.2 1.0 convert_multiply_fusion.4
  91.2 0.1 multiply_reduce_fusion.1
  91.3 0.1 fusion.69
  91.4 0.1 broadcast_multiply_fusion
  91.5 3.4 %fusion.39 = f32[8,4,1,128]{3,2,1,0:T(1,128)S(1)} fusion(f32[8,4,128,128]{3,2,1,0:T(8,128)} %param.38, f32[8,4,128,1]{2,0,1,3:T(8,128)S(1)} %fusion.69), kind=kOutput, calls=%fused_computation.62 | convolution fusion | flops 6291456 | bytes 2129920 | tf_op jit(solution)/shard_map/shd,shde->she/dot_general | solution.py:29
  94.9 0.1 multiply_bitcast_fusion
  95.0 0.8 multiply_add_fusion
  95.8 1.3 copy-done.2
  97.1 1.9 %fusion.37 = f32[8,4,1,128]{3,2,1,0:T(1,128)S(1)} fusion(f32[8,4,128,128]{3,2,1,0:T(8,128)S(1)} %multiply_add_fusion, f32[8,4,128,1]{2,0,1,3:T(8,128)S(1)} %get-tuple-element.12), kind=kOutput, calls=%fused_computation.60 | convolution fusion | flops 6291456 | bytes 2129920 | tf_op jit(solution)/shard_map/shd,shde->she/dot_general | solution.py:34
  99.0 0.1 fusion.31
  99.1 0.1 fusion.45
  99.2 13.1 %all_gather.14 = bf16[32,512]{1,0:T(8,128)(2,1)S(1)} all-gather(bf16[8,512]{1,0:T(8,128)(2,1)S(1)} %fusion.45), channel_id=1, replica_groups=mesh['dp'=4,'kv'=4,'tp'=2] {'kv'}, dimensions={0}, use_global_device_ids=true | all-gather | bytes 40960 | tf_op jit(solution)/shard_map/all_gather | solution.py:143
  112.3 0.8 convolution_convert_fusion.2
  113.2 5.8 %reduce-scatter.9.cloned.1.call-done = bf16[32,256]{1,0:T(8,128)(2,1)} async-done(((bf16[32,512]{1,0:T(8,128)(2,1)}), bf16[32,256]{1,0:T(8,128)(2,1)}) %reduce-scatter.9.cloned.1.call-update) | async-done | bytes 16400 | tf_op jit(solution)/shard_map/reduce_scatter | solution.py:147
  119.0 0.7 fusion.30
  119.7 14.2 %all_gather.15 = bf16[32,2048]{1,0:T(8,128)(2,1)S(1)} all-gather(bf16[32,256]{1,0:T(8,128)(2,1)S(1)} %fusion.30), channel_id=1, replica_groups=mesh['dp'=4,'kv'=4,'tp'=2] {'kv','tp'}, dimensions={1}, use_global_device_ids=true | all-gather | bytes 147456 | tf_op jit(solution)/shard_map/all_gather | solution.py:151
  133.9 0.1 fusion.5
  134.1 2.7 %fusion.22 = f32[32,704]{1,0:T(8,128)S(1)} fusion(bf16[2048,704]{0,1:T(8,128)(2,1)} %param.41, bf16[32,2048]{1,0:T(8,128)(2,1)S(1)} %all_gather.15, f32[2048]{0:T(1024)S(1)} %copy-done.6, f32[32]{0:T(128)S(1)} %add_rsqrt_fusion.3), kind=kOutput, calls=%fused_computation.40 | convolution fusion | flops 92536832 | bytes 3113088 | tf_op jit(solution)/shard_map/dot_general | solution.py:20
  136.8 5.1 %convolution_convert_fusion = bf16[32,2048]{1,0:T(8,128)(2,1)} fusion(bf16[704,2048]{1,0:T(8,128)(2,1)} %param.43, bf16[2048,704]{0,1:T(8,128)(2,1)} %param.42, f32[32,704]{1,0:T(8,128)S(1)} %fusion.22, bf16[32,2048]{1,0:T(8,128)(2,1)S(1)} %all_gather.15, f32[2048]{0:T(1024)S(1)} %copy-done.6, f32[32]{0:T(128)S(1)} %add_rsqrt_fusion.3), kind=kOutput, calls=%fused_computation | convolution fusion | flops 185012224 | bytes 6127744 | tf_op jit(solution)/shard_map/dot_general | solution.py:23
  141.9 31.6 %reduce-scatter.11.cloned.1.call-done = bf16[32,256]{1,0:T(8,128)(2,1)} async-done(((bf16[32,2048]{1,0:T(8,128)(2,1)}), bf16[32,256]{1,0:T(8,128)(2,1)}) %reduce-scatter.11.cloned.1.call-update) | async-done | bytes 16400 | tf_op jit(solution)/shard_map/reduce_scatter | solution.py:155
  173.5 1.3 add_convert_fusion
  (31 shorter events, 0.3 us)
Async XLA Ops:
  7.2 20.2 %copy-start = (bf16[704,2048]{1,0:T(8,128)(2,1)S(1)}, bf16[704,2048]{1,0:T(8,128)(2,1)}, u32[]{:S(2)}) copy-start(bf16[704,2048]{1,0:T(8,128)(2,1)} %param.26) | copy-start | bytes 8650756
  7.2 56.3 %reduce-scatter.5.cloned.1.call-start = ((), (), s32[]{:S(2)}) async-start(), calls=%async_computation.4 | async-start | bytes 147456 | tf_op jit(solution)/shard_map/reduce_scatter | solution.py:75
  23.5 0.5 copy-start.8
  27.4 36.2 %copy-start.5 = (bf16[32,256]{1,0:T(8,128)(2,1)S(1)}, bf16[32,256]{1,0:T(8,128)(2,1)}, u32[]{:S(2)}) copy-start(bf16[32,256]{1,0:T(8,128)(2,1)} %param.22) | copy-start | bytes 49156
  27.4 40.4 %copy-start.3 = (bf16[512,512]{1,0:T(8,128)(2,1)S(1)}, bf16[512,512]{1,0:T(8,128)(2,1)}, u32[]{:S(2)}) copy-start(bf16[512,512]{1,0:T(8,128)(2,1)} %param.29) | copy-start | bytes 1572868
  31.7 52.3 %copy-start.7 = (f32[8,4]{0,1:T(4,128)S(1)}, f32[8,4]{0,1:T(4,128)}, u32[]{:S(2)}) copy-start(f32[8,4]{0,1:T(4,128)} %param.36) | copy-start | bytes 388
  31.7 58.5 %reduce-scatter.7.cloned.1.call-start = ((), (), s32[]{:S(2)}) async-start(), calls=%async_computation.5 | async-start | bytes 163840 | tf_op jit(solution)/shard_map/reduce_scatter | solution.py:99
  72.4 46.6 %reduce-scatter.9.cloned.1.call-start = ((), (), s32[]{:S(2)}) async-start(), calls=%async_computation.6 | async-start | bytes 49152 | tf_op jit(solution)/shard_map/reduce_scatter | solution.py:147
  90.2 4.8 %copy-start.1 = (f32[8,4,128,128]{3,2,1,0:T(8,128)S(1)}, f32[8,4,128,128]{3,2,1,0:T(8,128)}, u32[]{:S(2)}) copy-start(f32[8,4,128,128]{3,2,1,0:T(8,128)} %param.38) | copy-start | bytes 6291460
  95.0 4.1 %copy-start.9 = (f32[128]{0:T(128)S(1)}, f32[128]{0:T(128)}, u32[]{:S(2)}) copy-start(f32[128]{0:T(128)} %param.37) | copy-start | bytes 1540
  95.0 17.3 %copy-start.4 = (bf16[512,512]{1,0:T(8,128)(2,1)S(1)}, bf16[512,512]{1,0:T(8,128)(2,1)}, u32[]{:S(2)}) copy-start(bf16[512,512]{1,0:T(8,128)(2,1)} %param.39) | copy-start | bytes 1572868
  95.0 39.0 %copy-start.6 = (f32[2048]{0:T(1024)S(1)}, f32[2048]{0:T(1024)}, u32[]{:S(2)}) copy-start(f32[2048]{0:T(1024)} %param.40) | copy-start | bytes 24580
  95.8 1.3 copy-start.2
  113.1 60.4 %reduce-scatter.11.cloned.1.call-start = ((), (), s32[]{:S(2)}) async-start(), calls=%async_computation.7 | async-start | bytes 147456 | tf_op jit(solution)/shard_map/reduce_scatter | solution.py:155
Sparse Core Ops, SparseCore 0:
  31.8 31.6 reduce-scatter.4
  72.5 17.6 reduce-scatter.6
  113.3 5.6 reduce-scatter.8
  142.0 31.4 reduce-scatter.10
